TPU v7x, 128 devices: a whole 4x4x4 slice. The times are simulated.
128 devices in a mesh: sp: 16 (over z, y), tp: 8 (over x, core).
Axes of the slice: x: 4, y: 4, z: 4, core: 2. Of those that a mesh axis runs over, the one named last changes fastest.
Arguments:
- tokens: bfloat16 [12288, 2048], P(('sp', 'tp')), may hold values from -6 to 6
- norm_gain: float32 [2048], replicated, may hold values from 0.1 to 1.9
- w_query: bfloat16 [2048, 1024], P('sp', 'tp'), may hold values from -0.125 to 0.125
- w_forget: bfloat16 [2048, 1024], P('sp', 'tp'), may hold values from -0.125 to 0.125
- w_input: bfloat16 [2048, 1024], P('sp', 'tp'), may hold values from -0.125 to 0.125
- w_outgate: bfloat16 [2048, 1024], P('sp', 'tp'), may hold values from -0.125 to 0.125
- w_conv_value: bfloat16 [2048, 1024], P('sp', 'tp'), may hold values from -0.125 to 0.125
- w_conv_gate: bfloat16 [2048, 1024], P('sp', 'tp'), may hold values from -0.125 to 0.125
- w_gate_rec: bfloat16 [2048, 2048], P('sp', 'tp'), may hold values from -0.125 to 0.125
- w_gate_conv: bfloat16 [2048, 2048], P('sp', 'tp'), may hold values from -0.125 to 0.125
- lower_bound: float32 [1024], P('tp'), may hold values from 0.92 to 0.9999593, as said below
- decay_shift: float32 [12288, 1024], P('sp', 'tp'), may hold values from -0.7 to 0, as said below
- state_init: float32 [8, 128, 128], P('tp'), may hold values from -0.125 to 0.125
- head_gain: float32 [1024], P('tp'), may hold values from 0.1 to 1.9
- conv_kernel: float32 [31, 1024], P(None, 'tp'), may hold values from -7.5 to 7.5
- channel_gain: float32 [1024], P('tp'), may hold values from 0.1 to 1.9
- channel_bias: float32 [1024], P('tp'), may hold values from -3 to 3
- w_out_rec: bfloat16 [1024, 2048], P('tp', 'sp'), may hold values from -0.1875 to 0.1875
- w_out_conv: bfloat16 [1024, 2048], P('tp', 'sp'), may hold values from -0.1875 to 0.1875
Outputs:
- mixed_out: bfloat16 [12288, 2048], P('sp', 'tp')
Inputs may be any that keep to these rules, and one draw needn't show every extreme that they name: `lower_bound`: every entry is below one. `decay_shift`: no entry is positive.
All inputs are finite; a program needn't handle non-finite values.
Results may differ from a plain program's by a relative error of at most 0.017.
Values may be sent and summed in bfloat16 or wider, within the bound.
A program may use at most 64 MiB of HBM per device.

v0:
```python
import jax
import jax.numpy as jnp
from jax import lax
from jax.sharding import PartitionSpec as P

HEAD = 128
CONV = 1024
KW = 31
BLOCK = 64
EPSILON = 1e-06


def in_one_piece(arrays, axis, dim, along):
    ends, at = ([], 0)
    for a in arrays[:-1]:
        at += a.shape[along]
        ends.append(at)
    both = jnp.concatenate(arrays, axis=along)
    return tuple(jnp.split(lax.all_gather(both, axis, axis=dim, tiled=True), ends, axis=along))


def sent_to_all(array, axis):
    size = lax.axis_size(axis)
    return lax.all_to_all(
        jnp.broadcast_to(array[None], (size, *array.shape)), axis, 0, 0, tiled=True
    )


def all_in_one(array, axis):
    leaves = jax.tree.leaves(array)
    sequence = sorted(range(len(leaves)), key=lambda k: -leaves[k].size)
    width = (1, *leaves[sequence[0]].shape)[-1]
    lines = [
        jnp.pad(leaves[k].reshape(-1), (0, -leaves[k].size % width)).reshape(-1, width)
        for k in sequence
    ]
    both, at, found = (sent_to_all(jnp.concatenate(lines), axis), 0, {})
    for k, line in zip(sequence, lines):
        section = both[:, at : at + len(line)].reshape(len(both), -1)
        found[k] = section[:, : leaves[k].size].reshape(-1, *leaves[k].shape)
        at += len(line)
    numbers = iter(range(len(leaves)))
    return jax.tree.map(lambda _: found[next(numbers)], array)


def joined_by_halves(pieces, combine):
    while len(jax.tree.leaves(pieces)[0]) > 1:
        pieces = jax.vmap(combine)(
            *(jax.tree.map(lambda part: part[side::2], pieces) for side in (0, 1))
        )
    return jax.tree.map(lambda part: part[0], pieces)


def entering(array, axis, combine, identity):
    size, position = (lax.axis_size(axis), lax.axis_index(axis))
    passed = jnp.arange(size) < position

    def kept(part, zero, own):
        part = jnp.where(
            passed.reshape(-1, *(1 for _ in own.shape)),
            part.astype(own.dtype),
            jnp.asarray(zero, own.dtype),
        )
        return part

    pieces = all_in_one(
        jax.tree.map(lambda part, kind: part.astype(kind), array, (jnp.bfloat16, jnp.bfloat16)),
        axis,
    )
    return joined_by_halves(jax.tree.map(kept, pieces, identity, array), combine)


def passed_along(block, axis, distance):
    devices = range(lax.axis_size(axis))
    route = [(i - distance, i) for i in devices if i - distance in devices]
    return lax.ppermute(block, axis, route)


def of_everyone(array, axis):
    everything = sent_to_all(array, axis)
    return jnp.sum(everything, axis=0)


def normalize_rows(values, gain_vector):
    widened = values.astype(jnp.float32)
    scale = lax.rsqrt(jnp.mean(widened * widened, axis=-1, keepdims=True) + EPSILON)
    return (widened * scale * gain_vector).astype(jnp.bfloat16)


def block_step(state, inputs):
    query, input_gate, values, log_decay = inputs
    length = query.shape[1]
    causal_masked = (jnp.arange(length)[:, None] >= jnp.arange(length)[None, :])[None, :, :, None]
    cumulative = jnp.cumsum(log_decay, axis=1)
    spread = cumulative[:, :, None, :] - cumulative[:, None, :, :]
    weight = jnp.where(causal_masked, jnp.exp(jnp.where(causal_masked, spread, 0.0)), 0.0)
    scores = jnp.einsum("htd,hsd,htsd->hts", query, input_gate, weight)
    output = jnp.einsum("hts,hsv->htv", scores, values)
    output = output + jnp.einsum("htd,hdv->htv", query * jnp.exp(cumulative), state)
    final = cumulative[:, -1:, :]
    carried = jnp.exp(final[:, 0, :])[:, :, None] * state
    carried = carried + jnp.einsum("hsd,hsv->hdv", input_gate * jnp.exp(final - cumulative), values)
    return (carried, output)


def compose(preceding_segment, later):
    return (preceding_segment[0] * later[0], later[0][..., None] * preceding_segment[1] + later[1])


def local(
    tokens,
    norm_gain,
    w_query,
    w_forget,
    w_input,
    w_outgate,
    w_conv_value,
    w_conv_gate,
    w_gate_rec,
    w_gate_conv,
    lower_bound,
    decay_shift,
    state_init,
    head_gain,
    conv_kernel,
    channel_gain,
    channel_bias,
    w_out_rec,
    w_out_conv,
):
    tp_count = lax.axis_size("tp")
    normed = normalize_rows(lax.all_gather(tokens, "tp", axis=0, tiled=True), norm_gain)
    row_count = normed.shape[0]
    weights = (
        w_query,
        w_forget,
        w_input,
        w_outgate,
        w_conv_value,
        w_conv_gate,
        w_gate_rec,
        w_gate_conv,
    )
    portions = in_one_piece(
        (
            weights[0],
            weights[1],
            weights[2],
            weights[3],
            weights[4],
            weights[5],
            weights[6],
            weights[7],
        ),
        "sp",
        0,
        1,
    )
    sums = tuple(
        (jnp.dot(normed, portion, preferred_element_type=jnp.float32) for portion in portions)
    )
    (
        query_raw,
        forget_raw,
        input_raw,
        outgate_raw,
        value_raw,
        gate_raw,
        gate_rec_raw,
        gate_conv_raw,
    ) = tuple((overall_aggregate.astype(jnp.bfloat16) for overall_aggregate in sums))
    local_heads = w_query.shape[1] // HEAD
    block_count = row_count // BLOCK
    query = jax.nn.silu(query_raw.astype(jnp.float32))
    input_gate = (1.0 - lower_bound) * jax.nn.sigmoid(-forget_raw.astype(jnp.float32))
    log_decay = jnp.log1p(-input_gate) + decay_shift
    values = input_raw.astype(jnp.float32)

    def to_blocks(array):
        return array.reshape(block_count, BLOCK, local_heads, HEAD).transpose(0, 2, 1, 3)

    zero_state = jnp.zeros((local_heads, HEAD, HEAD), jnp.float32)
    local_state, blocks_out = lax.scan(
        block_step,
        zero_state,
        (to_blocks(query), to_blocks(input_gate), to_blocks(values), to_blocks(log_decay)),
    )
    local_out = blocks_out.transpose(0, 2, 1, 3).reshape(row_count, local_heads, HEAD)
    running = jnp.cumsum(log_decay, axis=0)
    cumulated_forgetting = jnp.exp(running[-1]).reshape(local_heads, HEAD)
    ones_decay = jnp.ones_like(cumulated_forgetting)
    prefix_decay, prefix_state = entering(
        (cumulated_forgetting, local_state), "sp", compose, (ones_decay, zero_state)
    )
    incoming_state = prefix_decay[:, :, None] * state_init + prefix_state
    decayed_query = (query * jnp.exp(running)).reshape(row_count, local_heads, HEAD)
    head_out = local_out + jnp.einsum("thd,hdv->thv", decayed_query, incoming_state)
    head_out = head_out * lax.rsqrt(jnp.mean(head_out * head_out, axis=-1, keepdims=True) + EPSILON)
    head_out = head_out * head_gain.reshape(local_heads, HEAD)
    mixed_rec = (
        head_out.reshape(row_count, local_heads * HEAD)
        * jax.nn.silu(outgate_raw.astype(jnp.float32))
    ).astype(jnp.bfloat16)
    gated = (value_raw.astype(jnp.float32) * jax.nn.sigmoid(gate_raw.astype(jnp.float32))).astype(
        jnp.bfloat16
    )
    rim_width = KW - 1
    previous = passed_along(gated[row_count - rim_width :], "sp", 1)
    extended = jnp.concatenate([previous, gated], axis=0).astype(jnp.float32)
    conv_out = jnp.zeros((row_count, gated.shape[1]), jnp.float32)
    for tap_index in range(KW):
        conv_out = conv_out + conv_kernel[tap_index] * extended[tap_index : tap_index + row_count]
    squares = of_everyone(jnp.sum(conv_out * conv_out, axis=1), "tp")
    scale = lax.rsqrt(squares / CONV + EPSILON)[:, None]
    mixed_conv = jax.nn.silu(conv_out * scale * channel_gain + channel_bias).astype(jnp.bfloat16)
    rec_columns, conv_columns = in_one_piece((w_out_rec, w_out_conv), "sp", 1, 0)
    rec_width = mixed_rec.shape[1]
    rec_whole, conv_whole = in_one_piece((rec_columns, conv_columns), "tp", 0, 1)
    both = jnp.concatenate([mixed_rec, mixed_conv], axis=1).reshape(
        tp_count, row_count // tp_count, -1
    )
    arrived = lax.all_to_all(both, "tp", split_axis=0, concat_axis=2, tiled=True)
    item_count = arrived.shape[1]
    grouped = arrived.reshape(item_count, tp_count, -1)
    rec_part = grouped[:, :, :rec_width].reshape(item_count, -1)
    conv_part = grouped[:, :, rec_width:].reshape(item_count, -1)
    first = jnp.dot(rec_part, rec_whole, preferred_element_type=jnp.float32).astype(jnp.bfloat16)
    second = jnp.dot(conv_part, conv_whole, preferred_element_type=jnp.float32).astype(jnp.bfloat16)
    projected = jnp.stack([first, second], axis=1)[None]
    returned = lax.all_to_all(projected[0], "tp", split_axis=2, concat_axis=0, tiled=True)
    y_rec = returned[:, 0]
    y_conv = returned[:, 1]
    merged = jax.nn.sigmoid(gate_rec_raw.astype(jnp.float32)) * y_rec.astype(jnp.float32)
    merged = merged + jax.nn.sigmoid(gate_conv_raw.astype(jnp.float32)) * y_conv.astype(jnp.float32)
    return merged.astype(jnp.bfloat16)


def solution(mesh):
    in_specs = (
        P(("sp", "tp"), None),
        P(),
        P("sp", "tp"),
        P("sp", "tp"),
        P("sp", "tp"),
        P("sp", "tp"),
        P("sp", "tp"),
        P("sp", "tp"),
        P("sp", "tp"),
        P("sp", "tp"),
        P("tp"),
        P("sp", "tp"),
        P("tp", None, None),
        P("tp"),
        P(None, "tp"),
        P("tp"),
        P("tp"),
        P("tp", "sp"),
        P("tp", "sp"),
    )
    out_specs = P("sp", "tp")
    return jax.shard_map(local, mesh=mesh, in_specs=in_specs, out_specs=out_specs, check_vma=False)
```

profile of v0, /device:TPU:1, one launch (start us, length us, event | category | flops | bytes accessed | tf_op | source)
XLA Modules:
  0.0 333.0 jit_solution(5961914956780123622)
XLA Ops:
  16.6 1.6 slice_bitcast_fusion.35
  18.1 1.7 slice_bitcast_fusion.36
  19.8 34.6 %all-gather.9.cloned.1.call-done = bf16[256,2048]{1,0:T(8,128)(2,1)} async-done(((bf16[256,128]{1,0:T(8,128)(2,1)}), bf16[256,2048]{1,0:T(8,128)(2,1)}) %all-gather.9.cloned.1.call-update) | async-done | bytes 1048592 | tf_op jit(solution)/shard_map/all_gather | solution.py:19
  56.8 28.2 %all-gather.5.cloned.1.call-done = bf16[768,2048]{1,0:T(8,128)(2,1)} async-done(((bf16[96,2048]{1,0:T(8,128)(2,1)}), bf16[768,2048]{1,0:T(8,128)(2,1)}) %all-gather.5.cloned.1.call-update) | async-done | bytes 3145744 | tf_op jit(solution)/shard_map/all_gather | solution.py:132
  85.0 2.7 fusion.28
  88.6 54.3 %all-gather.7.cloned.1.call-done = bf16[2048,1280]{1,0:T(8,128)(2,1)} async-done(((bf16[128,1280]{1,0:T(8,128)(2,1)}), bf16[2048,1280]{1,0:T(8,128)(2,1)}) %all-gather.7.cloned.1.call-update) | async-done | bytes 5242896 | tf_op jit(solution)/shard_map/all_gather | solution.py:19
  142.9 2.8 divide_multiply_fusion
  145.7 2.1 convolution_convert_fusion.6
  147.7 2.9 log-plus-one_add_fusion
  150.7 80.2 %while.13 = (s32[]{:T(128)}, f32[1,128,128]{2,1,0:T(8,128)S(1)}, f32[12,1,64,128]{3,2,1,0:T(8,128)}, f32[12,1,64,128]{3,2,1,0:T(8,128)}, f32[12,1,64,128]{3,2,1,...) while((s32[]{:T(128)}, f32[1,128,128]{2,1,0:T(8,128)S(1)}, ...), condition=%wide.region_3.4_spmd.clone, body=%wide.region_1.3_spmd.clone.sunk | while | flops 9003011 | bytes 5051520 | solution.py:183
  153.0 1.7 fusion.167
  154.9 1.5 fusion.169
  159.7 1.7 fusion.167
  161.5 1.5 fusion.169
  166.3 1.7 fusion.167
  168.2 1.5 fusion.169
  173.0 1.7 fusion.167
  174.9 1.5 fusion.169
  179.7 1.7 fusion.167
  181.6 1.5 fusion.169
  186.4 1.7 fusion.167
  193.1 1.7 fusion.167
  199.8 1.7 fusion.167
  206.4 1.7 fusion.167
  208.3 1.5 fusion.169
  213.1 1.7 fusion.167
  215.0 1.5 fusion.169
  219.8 1.7 fusion.167
  221.7 1.5 fusion.169
  226.5 1.7 fusion.167
  228.4 1.5 fusion.169
  234.1 2.2 fusion.69
  236.5 2.0 fusion.68
  238.6 3.1 collective-permute-start
  245.3 5.5 %all-to-all-start.1 = ((f32[8,1,768]{2,1,0:T(1,128)}), f32[8,1,768]{2,1,0:T(1,128)}, u32[]{:S(2)}, u32[]{:S(2)}) async-start(f32[8,1,768]{2,1,0:T(1,128)} %broadcast_in_dim.89), calls=%async_computation.1 | async-start | bytes 49152 | tf_op jit(solution)/shard_map/all_to_all | solution.py:24
  252.2 3.4 %all-to-all-done.1 = f32[8,1,768]{2,1,0:T(1,128)} async-done(((f32[8,1,768]{2,1,0:T(1,128)}), f32[8,1,768]{2,1,0:T(1,128)}, u32[]{:S(2)}, u32[]{:S(2)}) %all-to-all-start.1) | async-done | bytes 24608 | tf_op jit(solution)/shard_map/all_to_all | solution.py:24
  255.6 1.6 broadcast_in_dim.85
  257.3 7.0 %all-to-all-start = ((bf16[16,129,128]{2,1,0:T(8,128)(2,1)}), bf16[16,129,128]{2,1,0:T(8,128)(2,1)}, u32[]{:S(2)}, u32[]{:S(2)}) async-start(bf16[16,129,128]{2,1,0:T(8,128)(2,1)} %broadcast_in_dim.85), calls=%async_computation | async-start | bytes 1114112 | tf_op jit(solution)/shard_map/all_to_all | solution.py:24
  265.1 1.5 multiply_convert_fusion
  266.6 8.4 %all-to-all-done = bf16[16,129,128]{2,1,0:T(8,128)(2,1)} async-done(((bf16[16,129,128]{2,1,0:T(8,128)(2,1)}), bf16[16,129,128]{2,1,0:T(8,128)(2,1)}, u32[]{:S(2)}, u32[]{:S(2)}) %all-to-all-start) | async-done | bytes 528416 | tf_op jit(solution)/shard_map/all_to_all | solution.py:24
  278.2 2.1 fusion.117
  280.3 12.6 %all_to_all.44 = bf16[8,96,256]{2,1,0:T(8,128)(2,1)S(1)} all-to-all(bf16[8,96,256]{2,1,0:T(8,128)(2,1)S(1)} %bitcast.263), channel_id=1, replica_groups=mesh['sp'=16,'tp'=8] {'tp'}, dimensions={0} | all-to-all | bytes 786432 | tf_op jit(solution)/shard_map/all_to_all | solution.py:222
  293.0 3.0 fusion.44
  296.0 3.0 fusion.41
  299.8 18.2 %all_to_all.45 = bf16[96,2,2048]{0,1,2:T(2,128)(2,1)S(1)} all-to-all(bf16[96,2,2048]{0,1,2:T(2,128)(2,1)S(1)} %copy.78), channel_id=1, replica_groups=mesh['sp'=16,'tp'=8] {'tp'}, dimensions={2} | all-to-all | bytes 1572864 | tf_op jit(solution)/shard_map/all_to_all | solution.py:230
  318.1 1.9 copy.79
  320.0 3.4 %fusion.60 = f32[768,256]{1,0:T(8,128)S(1)} fusion(bf16[768,2048]{1,0:T(8,128)(2,1)} %copy-done.1, bf16[2048,1280]{1,0:T(8,128)(2,1)} %all-gather.7.cloned.1.call-done, bf16[768,2,256]{2,0,1:T(8,128)(2,1)} %bitcast.268), kind=kOutput, calls=%fused_computation.65 | convolution fusion | flops 806682624 | bytes 5373952 | tf_op jit(solution)/shard_map/dot_general | solution.py:160
  323.5 3.0 fusion.54
  (251 shorter events, 71.7 us)
Async XLA Ops:
  6.5 47.8 %all-gather.9.cloned.1.call-start = ((), (), s32[]{:S(2)}) async-start(), calls=%async_computation.6 | async-start | bytes 1114112 | tf_op jit(solution)/shard_map/all_gather | solution.py:19
  8.0 77.0 %all-gather.5.cloned.1.call-start = ((), (), s32[]{:S(2)}) async-start(), calls=%async_computation.4 | async-start | bytes 3538944 | tf_op jit(solution)/shard_map/all_gather | solution.py:132
  8.7 134.1 %all-gather.7.cloned.1.call-start = ((), (), s32[]{:S(2)}) async-start(), calls=%async_computation.5 | async-start | bytes 5570560 | tf_op jit(solution)/shard_map/all_gather | solution.py:19
  15.8 277.2 %all-gather.11.cloned.1.call-start = ((), (), s32[]{:S(2)}) async-start(), calls=%async_computation.7 | async-start | bytes 9437184 | tf_op jit(solution)/shard_map/all_gather | solution.py:19
  55.7 32.0 %copy-start.12 = (f32[2048]{0:T(1024)S(1)}, f32[2048]{0:T(1024)}, u32[]{:S(2)}) copy-start(f32[2048]{0:T(1024)} %param.22) | copy-start | bytes 24580
  85.0 2.8 copy-start
  88.6 189.6 %copy-start.1 = (bf16[768,2048]{1,0:T(8,128)(2,1)}, bf16[768,2048]{1,0:T(8,128)(2,1)S(1)}, u32[]{:S(2)}) copy-start(bf16[768,2048]{1,0:T(8,128)(2,1)S(1)} %fusion.30) | copy-start | bytes 9437188
  145.7 2.1 copy-start.40
  232.1 0.8 copy-start.3
  234.1 8.2 %copy-start.4 = (f32[128,6,128]{0,2,1:T(8,128)}, f32[128,6,128]{0,2,1:T(8,128)S(1)}, u32[]{:S(2)}) copy-start(f32[128,6,128]{0,2,1:T(8,128)S(1)} %copy.72) | copy-start | bytes 1179652
  236.3 6.6 %copy-start.13 = (f32[128]{0:T(128)S(1)}, f32[128]{0:T(128)}, u32[]{:S(2)}) copy-start(f32[128]{0:T(128)} %get-tuple-element.149) | copy-start | bytes 1540
  236.3 6.6 %copy-start.14 = (f32[128]{0:T(128)S(1)}, f32[128]{0:T(128)}, u32[]{:S(2)}) copy-start(f32[128]{0:T(128)} %get-tuple-element.150) | copy-start | bytes 1540
  236.3 6.6 %copy-start.15 = (f32[128]{0:T(128)S(1)}, f32[128]{0:T(128)}, u32[]{:S(2)}) copy-start(f32[128]{0:T(128)} %get-tuple-element.151) | copy-start | bytes 1540
  236.3 6.6 %copy-start.16 = (f32[128]{0:T(128)S(1)}, f32[128]{0:T(128)}, u32[]{:S(2)}) copy-start(f32[128]{0:T(128)} %get-tuple-element.152) | copy-start | bytes 1540
  236.3 6.6 %copy-start.17 = (f32[128]{0:T(128)S(1)}, f32[128]{0:T(128)}, u32[]{:S(2)}) copy-start(f32[128]{0:T(128)} %get-tuple-element.153) | copy-start | bytes 1540
  236.3 6.6 %copy-start.18 = (f32[128]{0:T(128)S(1)}, f32[128]{0:T(128)}, u32[]{:S(2)}) copy-start(f32[128]{0:T(128)} %get-tuple-element.154) | copy-start | bytes 1540
  236.3 6.6 %copy-start.19 = (f32[128]{0:T(128)S(1)}, f32[128]{0:T(128)}, u32[]{:S(2)}) copy-start(f32[128]{0:T(128)} %get-tuple-element.155) | copy-start | bytes 1540
  236.3 6.6 %copy-start.20 = (f32[128]{0:T(128)S(1)}, f32[128]{0:T(128)}, u32[]{:S(2)}) copy-start(f32[128]{0:T(128)} %get-tuple-element.156) | copy-start | bytes 1540
  236.4 6.6 %copy-start.21 = (f32[128]{0:T(128)S(1)}, f32[128]{0:T(128)}, u32[]{:S(2)}) copy-start(f32[128]{0:T(128)} %get-tuple-element.126) | copy-start | bytes 1540
  236.4 6.6 %copy-start.22 = (f32[128]{0:T(128)S(1)}, f32[128]{0:T(128)}, u32[]{:S(2)}) copy-start(f32[128]{0:T(128)} %get-tuple-element.127) | copy-start | bytes 1540
  236.4 6.6 %copy-start.23 = (f32[128]{0:T(128)S(1)}, f32[128]{0:T(128)}, u32[]{:S(2)}) copy-start(f32[128]{0:T(128)} %get-tuple-element.128) | copy-start | bytes 1540
  236.4 6.6 %copy-start.24 = (f32[128]{0:T(128)S(1)}, f32[128]{0:T(128)}, u32[]{:S(2)}) copy-start(f32[128]{0:T(128)} %get-tuple-element.129) | copy-start | bytes 1540
  236.4 6.6 %copy-start.25 = (f32[128]{0:T(128)S(1)}, f32[128]{0:T(128)}, u32[]{:S(2)}) copy-start(f32[128]{0:T(128)} %get-tuple-element.130) | copy-start | bytes 1540
  236.4 6.6 %copy-start.26 = (f32[128]{0:T(128)S(1)}, f32[128]{0:T(128)}, u32[]{:S(2)}) copy-start(f32[128]{0:T(128)} %get-tuple-element.131) | copy-start | bytes 1540
  236.4 6.6 %copy-start.27 = (f32[128]{0:T(128)S(1)}, f32[128]{0:T(128)}, u32[]{:S(2)}) copy-start(f32[128]{0:T(128)} %get-tuple-element.132) | copy-start | bytes 1540
  236.4 6.6 %copy-start.28 = (f32[128]{0:T(128)S(1)}, f32[128]{0:T(128)}, u32[]{:S(2)}) copy-start(f32[128]{0:T(128)} %get-tuple-element.133) | copy-start | bytes 1540
  236.4 6.6 %copy-start.29 = (f32[128]{0:T(128)S(1)}, f32[128]{0:T(128)}, u32[]{:S(2)}) copy-start(f32[128]{0:T(128)} %get-tuple-element.134) | copy-start | bytes 1540
  236.4 6.6 %copy-start.30 = (f32[128]{0:T(128)S(1)}, f32[128]{0:T(128)}, u32[]{:S(2)}) copy-start(f32[128]{0:T(128)} %get-tuple-element.135) | copy-start | bytes 1540
  236.5 6.6 %copy-start.31 = (f32[128]{0:T(128)S(1)}, f32[128]{0:T(128)}, u32[]{:S(2)}) copy-start(f32[128]{0:T(128)} %get-tuple-element.136) | copy-start | bytes 1540
  236.5 6.6 %copy-start.32 = (f32[128]{0:T(128)S(1)}, f32[128]{0:T(128)}, u32[]{:S(2)}) copy-start(f32[128]{0:T(128)} %get-tuple-element.137) | copy-start | bytes 1540
  236.5 6.6 %copy-start.33 = (f32[128]{0:T(128)S(1)}, f32[128]{0:T(128)}, u32[]{:S(2)}) copy-start(f32[128]{0:T(128)} %get-tuple-element.138) | copy-start | bytes 1540
  236.5 6.6 %copy-start.34 = (f32[128]{0:T(128)S(1)}, f32[128]{0:T(128)}, u32[]{:S(2)}) copy-start(f32[128]{0:T(128)} %get-tuple-element.139) | copy-start | bytes 1540
  236.5 6.6 %copy-start.35 = (f32[128]{0:T(128)S(1)}, f32[128]{0:T(128)}, u32[]{:S(2)}) copy-start(f32[128]{0:T(128)} %get-tuple-element.140) | copy-start | bytes 1540
  236.5 6.6 %copy-start.36 = (f32[128]{0:T(128)S(1)}, f32[128]{0:T(128)}, u32[]{:S(2)}) copy-start(f32[128]{0:T(128)} %get-tuple-element.141) | copy-start | bytes 1540
  236.5 6.6 %copy-start.37 = (f32[128]{0:T(128)S(1)}, f32[128]{0:T(128)}, u32[]{:S(2)}) copy-start(f32[128]{0:T(128)} %get-tuple-element.142) | copy-start | bytes 1540
  236.5 6.6 %copy-start.38 = (f32[128]{0:T(128)S(1)}, f32[128]{0:T(128)}, u32[]{:S(2)}) copy-start(f32[128]{0:T(128)} %get-tuple-element.143) | copy-start | bytes 1540
  236.5 6.6 %copy-start.39 = (f32[128]{0:T(128)S(1)}, f32[128]{0:T(128)}, u32[]{:S(2)}) copy-start(f32[128]{0:T(128)} %get-tuple-element.144) | copy-start | bytes 1540
  238.6 4.3 %collective-permute-start = (bf16[30,128]{1,0:T(8,128)(2,1)S(1)}, bf16[30,128]{1,0:T(8,128)(2,1)S(1)}, u32[]{:S(2)}, u32[]{:S(2)}) collective-permute-start(bf16[30,128]{1,0:T(8,128)(2,1)S(1)} %slice.369), channel_id=1, source_target_pairs={{0,8},{8,16},{16,24},{24,32},{32,40},{40,48},{48,56},{56,64},{64,7... | collective-permute-start | bytes 23048 | tf_op jit(solution)/shard_map/ppermute | solution.py:76
  245.3 10.3 %all-to-all-start.1 = ((f32[8,1,768]{2,1,0:T(1,128)}), f32[8,1,768]{2,1,0:T(1,128)}, u32[]{:S(2)}, u32[]{:S(2)}) async-start(f32[8,1,768]{2,1,0:T(1,128)} %broadcast_in_dim.89), calls=%async_computation.1 | async-start | bytes 49152 | tf_op jit(solution)/shard_map/all_to_all | solution.py:24
  257.3 17.8 %all-to-all-start = ((bf16[16,129,128]{2,1,0:T(8,128)(2,1)}), bf16[16,129,128]{2,1,0:T(8,128)(2,1)}, u32[]{:S(2)}, u32[]{:S(2)}) async-start(bf16[16,129,128]{2,1,0:T(8,128)(2,1)} %broadcast_in_dim.85), calls=%async_computation | async-start | bytes 1114112 | tf_op jit(solution)/shard_map/all_to_all | solution.py:24
  266.6 11.1 %copy-start.5 = (f32[128,6,128]{0,2,1:T(8,128)S(1)}, f32[128,6,128]{0,2,1:T(8,128)}, u32[]{:S(2)}) copy-start(f32[128,6,128]{0,2,1:T(8,128)} %copy-done.4) | copy-start | bytes 1179652
  266.6 11.5 %copy-start.41 = (f32[128]{0:T(128)S(1)}, f32[128]{0:T(128)}, u32[]{:S(2)}) copy-start(f32[128]{0:T(128)} %param.34) | copy-start | bytes 1540
  275.1 2.6 copy-start.6
  275.1 2.6 copy-start.10
  275.1 2.7 copy-start.11
  278.2 2.1 copy-start.8
  320.0 3.4 %copy-start.2 = (bf16[768,2048]{1,0:T(8,128)(2,1)S(1)}, bf16[768,2048]{1,0:T(8,128)(2,1)}, u32[]{:S(2)}) copy-start(bf16[768,2048]{1,0:T(8,128)(2,1)} %copy-done.1) | copy-start | bytes 9437188
  320.0 3.5 %copy-start.7 = (bf16[96,2,8,256]{3,0,2,1:T(8,128)(2,1)S(1)}, bf16[96,2,8,256]{3,0,2,1:T(8,128)(2,1)}, u32[]{:S(2)}) copy-start(bf16[96,2,8,256]{3,0,2,1:T(8,128)(2,1)} %copy.79) | copy-start | bytes 2359300
  (1 other events, 0.7 us)
Sparse Core Ops, SparseCore 0:
  9.4 44.8 all-gather.8
  56.0 28.8 all-gather.4
  87.1 55.7 all-gather.6
  144.4 49.7 all-gather.10
where the time goes:
time: 338 us; the launch traced here: 333 us
  waiting for transfers between devices  130 us (38%)
  matrix products  58.7 us (17%)
  other arithmetic  47.2 us (14%)
  local copies, waits for them, and re-layouts  36.5 us (11%)
  blocking collectives  30.8 us (9%)
  starting transfers between devices  15.8 us (5%)
  between operations  13.9 us (4%)
    all_gather x3, waiting for transfers between devices, in_one_piece(): lax.all_gather(both, axis, axis=dim, tiled=True)  88.9 us
    all_gather x1, waiting for transfers between devices, local(): lax.all_gather(tokens, 'tp', axis=0, tiled=True)  28.2 us
    dot_general x12, other arithmetic, block_step(): scores = jnp.einsum('htd,hsd,htsd->hts', query, input_gate, weight)  20.5 us
    dot_general x8, matrix products, local(): jnp.dot(normed, portion, preferred_element_type=jnp.float32)  20.5 us
    all_to_all x1, blocking collectives, local(): lax.all_to_all(projected[0], 'tp', split_axis=2, concat_axis=0, tiled=True)  18.2 us
    dot_general x12, matrix products, block_step(): jnp.einsum('htd,hdv->htv', query * jnp.exp(cumulative), state)  18.2 us
    all_to_all x2, starting transfers between devices, sent_to_all(): lax.all_to_all(jnp.broadcast_to(array[None], (size, *array.shape)), axis,...  12.6 us
    all_to_all x1, blocking collectives, local(): lax.all_to_all(both, 'tp', split_axis=0, concat_axis=2, tiled=True)  12.6 us
  transfers between devices with their start and end apart: 7, of which 5 were waited for; matrix products, arithmetic and copies ran while one was open for 37% of the time, Pallas kernels for 0%

commit v1 on v0

--- a/solution.py
+++ b/solution.py
@@ -8,6 +8,27 @@
 KW = 31
 BLOCK = 64
 EPSILON = 1e-06
+
+
+def gather_around(x, axis, dim):
+    peers, mine, rows = (lax.axis_size(axis), lax.axis_index(axis), x.shape[dim])
+    forward = [(i, (i + 1) % peers) for i in range(peers)]
+    left = [(i, (i - 1) % peers) for i in range(peers)]
+    out = jnp.zeros((*x.shape[:dim], peers * rows, *x.shape[dim + 1 :]), x.dtype)
+    out = lax.dynamic_update_slice_in_dim(out, x, mine * rows, axis=dim)
+    from_left = from_right = x
+    half = peers // 2
+    for step in range(1, half + 1):
+        from_left = lax.ppermute(from_left, axis, forward)
+        out = lax.dynamic_update_slice_in_dim(
+            out, from_left, (mine - step) % peers * rows, axis=dim
+        )
+        if step < peers - half:
+            from_right = lax.ppermute(from_right, axis, left)
+            out = lax.dynamic_update_slice_in_dim(
+                out, from_right, (mine + step) % peers * rows, axis=dim
+            )
+    return out
 
 
 def in_one_piece(arrays, axis, dim, along):
@@ -129,7 +150,7 @@
     w_out_conv,
 ):
     tp_count = lax.axis_size("tp")
-    normed = normalize_rows(lax.all_gather(tokens, "tp", axis=0, tiled=True), norm_gain)
+    normed = normalize_rows(gather_around(tokens, "tp", 0), norm_gain)
     row_count = normed.shape[0]
     weights = (
         w_query,

time: 338 us -> 307 us (0.908)
  waiting for transfers between devices: 130 us -> 91 us
  starting transfers between devices: 15.8 us -> 26.5 us
    all_gather x1 -> x0, waiting for transfers between devices: 28.2 us -> none  [local(): lax.all_gather(tokens, 'tp', axis=0, tiled=True)]
    all_gather x3, waiting for transfers between devices: 88.9 us -> 65.3 us  [in_one_piece(): lax.all_gather(both, axis, axis=dim, tiled=True)]
    ppermute x0 -> x7, waiting for transfers between devices: none -> 13.8 us  [the longest x4 12.8 us: gather_around(): from_left = lax.ppermute(from_left, axis, forward)]
    ppermute x0 -> x7, starting transfers between devices: none -> 10.8 us  [the longest x4 9.93 us: gather_around(): from_left = lax.ppermute(from_left, axis, forward)]
    unnamed x92 -> x90, local copies, waits for them, and re-layouts: 7.34 us -> 7.22 us
  transfers between devices with their start and end apart: 7 -> 13, of which waited for: 5 -> 10; matrix products, arithmetic and copies ran while one was open for 37% -> 41% of each run, Pallas kernels for 0% -> 0%
where the time goes in v1:
time: 307 us; the launch traced here: 302 us
  waiting for transfers between devices  91 us (30%)
  matrix products  58.6 us (19%)
  other arithmetic  45.2 us (15%)
  local copies, waits for them, and re-layouts  35.9 us (12%)
  blocking collectives  30.8 us (10%)
  starting transfers between devices  26.5 us (9%)
  between operations  14 us (5%)
    all_gather x3, waiting for transfers between devices, in_one_piece(): lax.all_gather(both, axis, axis=dim, tiled=True)  65.3 us
    dot_general x12, other arithmetic, block_step(): scores = jnp.einsum('htd,hsd,htsd->hts', query, input_gate, weight)  20.5 us
    dot_general x8, matrix products, local(): jnp.dot(normed, portion, preferred_element_type=jnp.float32)  20.4 us
    all_to_all x1, blocking collectives, local(): lax.all_to_all(projected[0], 'tp', split_axis=2, concat_axis=0, tiled=True)  18.2 us
    dot_general x12, matrix products, block_step(): jnp.einsum('htd,hdv->htv', query * jnp.exp(cumulative), state)  18.2 us
    ppermute x4, waiting for transfers between devices, gather_around(): from_left = lax.ppermute(from_left, axis, forward)  12.8 us
    all_to_all x1, blocking collectives, local(): lax.all_to_all(both, 'tp', split_axis=0, concat_axis=2, tiled=True)  12.5 us
    all_to_all x2, starting transfers between devices, sent_to_all(): lax.all_to_all(jnp.broadcast_to(array[None], (size, *array.shape)), axis,...  12.4 us
  transfers between devices with their start and end apart: 13, of which 10 were waited for; matrix products, arithmetic and copies ran while one was open for 41% of the time, Pallas kernels for 0%

profile of v1, /device:TPU:1, one launch (start us, length us, event | category | flops | bytes accessed | tf_op | source)
XLA Modules:
  0.0 302.4 jit_solution(7100822343950329148)
XLA Ops:
  15.2 2.6 collective-permute-start
  17.8 1.6 slice_bitcast_fusion.35
  19.3 1.6 slice_bitcast_fusion.36
  22.8 2.4 collective-permute-start.2
  25.3 4.6 %collective-permute-done.2 = bf16[96,2048]{1,0:T(8,128)(2,1)S(1)} collective-permute-done((bf16[96,2048]{1,0:T(8,128)(2,1)S(1)}, bf16[96,2048]{1,0:T(8,128)(2,1)S(1)}, u32[]{:S(2)}, u32[]{:S(2)}) %collective-permute-start.2) | collective-permute-done | bytes 393248 | tf_op jit(solution)/shard_map/ppermute | solution.py:22
  29.9 2.5 collective-permute-start.4
  33.7 3.4 %collective-permute-done.4 = bf16[96,2048]{1,0:T(8,128)(2,1)S(1)} collective-permute-done((bf16[96,2048]{1,0:T(8,128)(2,1)S(1)}, bf16[96,2048]{1,0:T(8,128)(2,1)S(1)}, u32[]{:S(2)}, u32[]{:S(2)}) %collective-permute-start.4) | collective-permute-done | bytes 393248 | tf_op jit(solution)/shard_map/ppermute | solution.py:22
  37.1 2.5 collective-permute-start.6
  40.3 4.0 %collective-permute-done.6 = bf16[96,2048]{1,0:T(8,128)(2,1)S(1)} collective-permute-done((bf16[96,2048]{1,0:T(8,128)(2,1)S(1)}, bf16[96,2048]{1,0:T(8,128)(2,1)S(1)}, u32[]{:S(2)}, u32[]{:S(2)}) %collective-permute-start.6) | collective-permute-done | bytes 393248 | tf_op jit(solution)/shard_map/ppermute | solution.py:22
  45.9 8.5 %all-gather.6.cloned.1.call-done = bf16[256,2048]{1,0:T(8,128)(2,1)} async-done(((bf16[256,128]{1,0:T(8,128)(2,1)}), bf16[256,2048]{1,0:T(8,128)(2,1)}) %all-gather.6.cloned.1.call-update) | async-done | bytes 1048592 | tf_op jit(solution)/shard_map/all_gather | solution.py:40
  56.8 56.8 %all-gather.4.cloned.1.call-done = bf16[2048,1280]{1,0:T(8,128)(2,1)} async-done(((bf16[128,1280]{1,0:T(8,128)(2,1)}), bf16[2048,1280]{1,0:T(8,128)(2,1)}) %all-gather.4.cloned.1.call-update) | async-done | bytes 5242896 | tf_op jit(solution)/shard_map/all_gather | solution.py:40
  113.5 2.8 divide_multiply_fusion
  116.3 2.1 convolution_convert_fusion.6
  118.4 2.9 log-plus-one_add_fusion
  121.4 80.2 %while.13 = (s32[]{:T(128)}, f32[1,128,128]{2,1,0:T(8,128)S(1)}, f32[12,1,64,128]{3,2,1,0:T(8,128)}, f32[12,1,64,128]{3,2,1,0:T(8,128)}, f32[12,1,64,128]{3,2,1,...) while((s32[]{:T(128)}, f32[1,128,128]{2,1,0:T(8,128)S(1)}, ...), condition=%wide.region_3.4_spmd.clone, body=%wide.region_1.3_spmd.clone.sunk | while | flops 9003011 | bytes 5051520 | solution.py:204
  123.6 1.7 fusion.167
  125.5 1.5 fusion.169
  130.3 1.7 fusion.167
  132.2 1.5 fusion.169
  137.0 1.7 fusion.167
  138.9 1.5 fusion.169
  143.7 1.7 fusion.167
  145.6 1.5 fusion.169
  150.4 1.7 fusion.167
  152.3 1.5 fusion.169
  157.1 1.7 fusion.167
  163.7 1.7 fusion.167
  170.4 1.7 fusion.167
  177.1 1.7 fusion.167
  183.8 1.7 fusion.167
  190.4 1.7 fusion.167
  197.1 1.7 fusion.167
  204.8 2.2 fusion.66
  207.2 2.0 fusion.69
  209.2 3.3 %collective-permute-start.7 = (bf16[30,128]{1,0:T(8,128)(2,1)S(1)}, bf16[30,128]{1,0:T(8,128)(2,1)S(1)}, u32[]{:S(2)}, u32[]{:S(2)}) collective-permute-start(bf16[30,128]{1,0:T(8,128)(2,1)S(1)} %slice.369), channel_id=1, source_target_pairs={{0,8},{8,16},{16,24},{24,32},{32,40},{40,48},{48,56},{56,64},{64,7... | collective-permute-start | bytes 23048 | tf_op jit(solution)/shard_map/ppermute | solution.py:97
  216.2 5.4 %all-to-all-start.1 = ((f32[8,1,768]{2,1,0:T(1,128)}), f32[8,1,768]{2,1,0:T(1,128)}, u32[]{:S(2)}, u32[]{:S(2)}) async-start(f32[8,1,768]{2,1,0:T(1,128)} %broadcast_in_dim.93), calls=%async_computation.1 | async-start | bytes 49152 | tf_op jit(solution)/shard_map/all_to_all | solution.py:45
  222.9 3.4 %all-to-all-done.1 = f32[8,1,768]{2,1,0:T(1,128)} async-done(((f32[8,1,768]{2,1,0:T(1,128)}), f32[8,1,768]{2,1,0:T(1,128)}, u32[]{:S(2)}, u32[]{:S(2)}) %all-to-all-start.1) | async-done | bytes 24608 | tf_op jit(solution)/shard_map/all_to_all | solution.py:45
  226.3 1.7 broadcast_in_dim.89
  228.0 7.0 %all-to-all-start = ((bf16[16,129,128]{2,1,0:T(8,128)(2,1)}), bf16[16,129,128]{2,1,0:T(8,128)(2,1)}, u32[]{:S(2)}, u32[]{:S(2)}) async-start(bf16[16,129,128]{2,1,0:T(8,128)(2,1)} %broadcast_in_dim.89), calls=%async_computation | async-start | bytes 1114112 | tf_op jit(solution)/shard_map/all_to_all | solution.py:45
  235.8 1.5 multiply_convert_fusion
  237.3 8.4 %all-to-all-done = bf16[16,129,128]{2,1,0:T(8,128)(2,1)} async-done(((bf16[16,129,128]{2,1,0:T(8,128)(2,1)}), bf16[16,129,128]{2,1,0:T(8,128)(2,1)}, u32[]{:S(2)}, u32[]{:S(2)}) %all-to-all-start) | async-done | bytes 528416 | tf_op jit(solution)/shard_map/all_to_all | solution.py:45
  248.9 2.1 fusion.117
  251.0 12.5 %all_to_all.44 = bf16[8,96,256]{2,1,0:T(8,128)(2,1)S(1)} all-to-all(bf16[8,96,256]{2,1,0:T(8,128)(2,1)S(1)} %bitcast.263), channel_id=1, replica_groups=mesh['sp'=16,'tp'=8] {'tp'}, dimensions={0} | all-to-all | bytes 786432 | tf_op jit(solution)/shard_map/all_to_all | solution.py:243
  263.7 3.0 fusion.44
  266.7 3.0 fusion.41
  270.5 18.2 %all_to_all.45 = bf16[96,2,2048]{0,1,2:T(2,128)(2,1)S(1)} all-to-all(bf16[96,2,2048]{0,1,2:T(2,128)(2,1)S(1)} %copy.78), channel_id=1, replica_groups=mesh['sp'=16,'tp'=8] {'tp'}, dimensions={2} | all-to-all | bytes 1572864 | tf_op jit(solution)/shard_map/all_to_all | solution.py:251
  289.5 3.3 %fusion.60 = f32[768,256]{1,0:T(8,128)S(1)} fusion(bf16[768,2048]{1,0:T(8,128)(2,1)} %copy-done, bf16[2048,1280]{1,0:T(8,128)(2,1)} %all-gather.4.cloned.1.call-done, bf16[768,2,256]{2,0,1:T(8,128)(2,1)S(1)} %bitcast.268), kind=kOutput, calls=%fused_computation.65 | convolution fusion | flops 806682624 | bytes 5373952 | tf_op jit(solution)/shard_map/dot_general | solution.py:181
  292.9 3.0 fusion.54
  (269 shorter events, 81.6 us)
Async XLA Ops:
  6.5 15.5 %copy-start.8 = (bf16[96,2048]{1,0:T(8,128)(2,1)S(1)}, bf16[96,2048]{1,0:T(8,128)(2,1)}, u32[]{:S(2)}) copy-start(bf16[96,2048]{1,0:T(8,128)(2,1)} %param.21) | copy-start | bytes 1179652
  6.5 47.8 %all-gather.6.cloned.1.call-start = ((), (), s32[]{:S(2)}) async-start(), calls=%async_computation.5 | async-start | bytes 1114112 | tf_op jit(solution)/shard_map/all_gather | solution.py:40
  8.0 105.5 %all-gather.4.cloned.1.call-start = ((), (), s32[]{:S(2)}) async-start(), calls=%async_computation.4 | async-start | bytes 5570560 | tf_op jit(solution)/shard_map/all_gather | solution.py:40
  15.1 248.6 %all-gather.8.cloned.1.call-start = ((), (), s32[]{:S(2)}) async-start(), calls=%async_computation.6 | async-start | bytes 9437184 | tf_op jit(solution)/shard_map/all_gather | solution.py:40
  15.2 7.6 %collective-permute-start = (bf16[96,2048]{1,0:T(8,128)(2,1)}, bf16[96,2048]{1,0:T(8,128)(2,1)S(1)}, u32[]{:S(2)}, u32[]{:S(2)}) collective-permute-start(bf16[96,2048]{1,0:T(8,128)(2,1)} %param.21), channel_id=1, source_target_pairs={{0,1},{1,2},{2,3},{3,4},{4,5},{5,6},{6,7},{7,0},{8,9},{9,10},{10,1... | collective-permute-start | bytes 1179656 | tf_op jit(solution)/shard_map/ppermute | solution.py:22
  17.8 7.4 %collective-permute-start.1 = (bf16[96,2048]{1,0:T(8,128)(2,1)}, bf16[96,2048]{1,0:T(8,128)(2,1)S(1)}, u32[]{:S(2)}, u32[]{:S(2)}) collective-permute-start(bf16[96,2048]{1,0:T(8,128)(2,1)} %param.21), channel_id=1, source_target_pairs={{0,7},{1,0},{2,1},{3,2},{4,3},{5,4},{6,5},{7,6},{8,15},{9,8},{10,9... | collective-permute-start | bytes 1179656 | tf_op jit(solution)/shard_map/ppermute | solution.py:27
  22.8 7.1 %collective-permute-start.2 = (bf16[96,2048]{1,0:T(8,128)(2,1)S(1)}, bf16[96,2048]{1,0:T(8,128)(2,1)S(1)}, u32[]{:S(2)}, u32[]{:S(2)}) collective-permute-start(bf16[96,2048]{1,0:T(8,128)(2,1)S(1)} %collective-permute-done), channel_id=1, source_target_pairs={{0,1},{1,2},{2,3},{3,4},{4,5},{5,6},{6,7},{7,0},{8,9},{9,10},{10,1... | collective-permute-start | bytes 1179656 | tf_op jit(solution)/shard_map/ppermute | solution.py:22
  25.2 7.6 %collective-permute-start.3 = (bf16[96,2048]{1,0:T(8,128)(2,1)S(1)}, bf16[96,2048]{1,0:T(8,128)(2,1)S(1)}, u32[]{:S(2)}, u32[]{:S(2)}) collective-permute-start(bf16[96,2048]{1,0:T(8,128)(2,1)S(1)} %collective-permute-done.1), channel_id=1, source_target_pairs={{0,7},{1,0},{2,1},{3,2},{4,3},{5,4},{6,5},{7,6},{8,15},{9,8},{10,9... | collective-permute-start | bytes 1179656 | tf_op jit(solution)/shard_map/ppermute | solution.py:27
  29.9 7.2 %collective-permute-start.4 = (bf16[96,2048]{1,0:T(8,128)(2,1)S(1)}, bf16[96,2048]{1,0:T(8,128)(2,1)S(1)}, u32[]{:S(2)}, u32[]{:S(2)}) collective-permute-start(bf16[96,2048]{1,0:T(8,128)(2,1)S(1)} %collective-permute-done.2), channel_id=1, source_target_pairs={{0,1},{1,2},{2,3},{3,4},{4,5},{5,6},{6,7},{7,0},{8,9},{9,10},{10,1... | collective-permute-start | bytes 1179656 | tf_op jit(solution)/shard_map/ppermute | solution.py:22
  32.8 7.5 %collective-permute-start.5 = (bf16[96,2048]{1,0:T(8,128)(2,1)S(1)}, bf16[96,2048]{1,0:T(8,128)(2,1)S(1)}, u32[]{:S(2)}, u32[]{:S(2)}) collective-permute-start(bf16[96,2048]{1,0:T(8,128)(2,1)S(1)} %collective-permute-done.3), channel_id=1, source_target_pairs={{0,7},{1,0},{2,1},{3,2},{4,3},{5,4},{6,5},{7,6},{8,15},{9,8},{10,9... | collective-permute-start | bytes 1179656 | tf_op jit(solution)/shard_map/ppermute | solution.py:27
  33.6 11.4 %copy-start.11 = (f32[2048]{0:T(1024)S(1)}, f32[2048]{0:T(1024)}, u32[]{:S(2)}) copy-start(f32[2048]{0:T(1024)} %param.22) | copy-start | bytes 24580
  37.1 7.2 %collective-permute-start.6 = (bf16[96,2048]{1,0:T(8,128)(2,1)S(1)}, bf16[96,2048]{1,0:T(8,128)(2,1)S(1)}, u32[]{:S(2)}, u32[]{:S(2)}) collective-permute-start(bf16[96,2048]{1,0:T(8,128)(2,1)S(1)} %collective-permute-done.4), channel_id=1, source_target_pairs={{0,1},{1,2},{2,3},{3,4},{4,5},{5,6},{6,7},{7,0},{8,9},{9,10},{10,1... | collective-permute-start | bytes 1179656 | tf_op jit(solution)/shard_map/ppermute | solution.py:22
  45.8 203.0 %copy-start = (bf16[768,2048]{1,0:T(8,128)(2,1)}, bf16[768,2048]{1,0:T(8,128)(2,1)S(1)}, u32[]{:S(2)}) copy-start(bf16[768,2048]{1,0:T(8,128)(2,1)S(1)} %fusion.30) | copy-start | bytes 9437188
  204.8 8.4 %copy-start.3 = (f32[128,6,128]{0,2,1:T(8,128)}, f32[128,6,128]{0,2,1:T(8,128)S(1)}, u32[]{:S(2)}) copy-start(f32[128,6,128]{0,2,1:T(8,128)S(1)} %copy.72) | copy-start | bytes 1179652
  206.9 6.8 %copy-start.12 = (f32[128]{0:T(128)S(1)}, f32[128]{0:T(128)}, u32[]{:S(2)}) copy-start(f32[128]{0:T(128)} %get-tuple-element.149) | copy-start | bytes 1540
  207.0 6.8 %copy-start.13 = (f32[128]{0:T(128)S(1)}, f32[128]{0:T(128)}, u32[]{:S(2)}) copy-start(f32[128]{0:T(128)} %get-tuple-element.150) | copy-start | bytes 1540
  207.0 6.8 %copy-start.14 = (f32[128]{0:T(128)S(1)}, f32[128]{0:T(128)}, u32[]{:S(2)}) copy-start(f32[128]{0:T(128)} %get-tuple-element.151) | copy-start | bytes 1540
  207.0 6.8 %copy-start.15 = (f32[128]{0:T(128)S(1)}, f32[128]{0:T(128)}, u32[]{:S(2)}) copy-start(f32[128]{0:T(128)} %get-tuple-element.152) | copy-start | bytes 1540
  207.0 6.8 %copy-start.16 = (f32[128]{0:T(128)S(1)}, f32[128]{0:T(128)}, u32[]{:S(2)}) copy-start(f32[128]{0:T(128)} %get-tuple-element.153) | copy-start | bytes 1540
  207.0 6.8 %copy-start.17 = (f32[128]{0:T(128)S(1)}, f32[128]{0:T(128)}, u32[]{:S(2)}) copy-start(f32[128]{0:T(128)} %get-tuple-element.154) | copy-start | bytes 1540
  207.0 6.8 %copy-start.18 = (f32[128]{0:T(128)S(1)}, f32[128]{0:T(128)}, u32[]{:S(2)}) copy-start(f32[128]{0:T(128)} %get-tuple-element.155) | copy-start | bytes 1540
  207.0 6.8 %copy-start.19 = (f32[128]{0:T(128)S(1)}, f32[128]{0:T(128)}, u32[]{:S(2)}) copy-start(f32[128]{0:T(128)} %get-tuple-element.156) | copy-start | bytes 1540
  207.0 6.8 %copy-start.20 = (f32[128]{0:T(128)S(1)}, f32[128]{0:T(128)}, u32[]{:S(2)}) copy-start(f32[128]{0:T(128)} %get-tuple-element.126) | copy-start | bytes 1540
  207.0 6.8 %copy-start.21 = (f32[128]{0:T(128)S(1)}, f32[128]{0:T(128)}, u32[]{:S(2)}) copy-start(f32[128]{0:T(128)} %get-tuple-element.127) | copy-start | bytes 1540
  207.0 6.8 %copy-start.22 = (f32[128]{0:T(128)S(1)}, f32[128]{0:T(128)}, u32[]{:S(2)}) copy-start(f32[128]{0:T(128)} %get-tuple-element.128) | copy-start | bytes 1540
  207.1 6.8 %copy-start.23 = (f32[128]{0:T(128)S(1)}, f32[128]{0:T(128)}, u32[]{:S(2)}) copy-start(f32[128]{0:T(128)} %get-tuple-element.129) | copy-start | bytes 1540
  207.1 6.8 %copy-start.24 = (f32[128]{0:T(128)S(1)}, f32[128]{0:T(128)}, u32[]{:S(2)}) copy-start(f32[128]{0:T(128)} %get-tuple-element.130) | copy-start | bytes 1540
  207.1 6.8 %copy-start.25 = (f32[128]{0:T(128)S(1)}, f32[128]{0:T(128)}, u32[]{:S(2)}) copy-start(f32[128]{0:T(128)} %get-tuple-element.131) | copy-start | bytes 1540
  207.1 6.8 %copy-start.26 = (f32[128]{0:T(128)S(1)}, f32[128]{0:T(128)}, u32[]{:S(2)}) copy-start(f32[128]{0:T(128)} %get-tuple-element.132) | copy-start | bytes 1540
  207.1 6.8 %copy-start.27 = (f32[128]{0:T(128)S(1)}, f32[128]{0:T(128)}, u32[]{:S(2)}) copy-start(f32[128]{0:T(128)} %get-tuple-element.133) | copy-start | bytes 1540
  207.1 6.8 %copy-start.28 = (f32[128]{0:T(128)S(1)}, f32[128]{0:T(128)}, u32[]{:S(2)}) copy-start(f32[128]{0:T(128)} %get-tuple-element.134) | copy-start | bytes 1540
  207.1 6.8 %copy-start.29 = (f32[128]{0:T(128)S(1)}, f32[128]{0:T(128)}, u32[]{:S(2)}) copy-start(f32[128]{0:T(128)} %get-tuple-element.135) | copy-start | bytes 1540
  207.1 6.8 %copy-start.30 = (f32[128]{0:T(128)S(1)}, f32[128]{0:T(128)}, u32[]{:S(2)}) copy-start(f32[128]{0:T(128)} %get-tuple-element.136) | copy-start | bytes 1540
  207.1 6.8 %copy-start.31 = (f32[128]{0:T(128)S(1)}, f32[128]{0:T(128)}, u32[]{:S(2)}) copy-start(f32[128]{0:T(128)} %get-tuple-element.137) | copy-start | bytes 1540
  207.1 6.8 %copy-start.32 = (f32[128]{0:T(128)S(1)}, f32[128]{0:T(128)}, u32[]{:S(2)}) copy-start(f32[128]{0:T(128)} %get-tuple-element.138) | copy-start | bytes 1540
  207.2 6.8 %copy-start.33 = (f32[128]{0:T(128)S(1)}, f32[128]{0:T(128)}, u32[]{:S(2)}) copy-start(f32[128]{0:T(128)} %get-tuple-element.139) | copy-start | bytes 1540
  207.2 6.8 %copy-start.34 = (f32[128]{0:T(128)S(1)}, f32[128]{0:T(128)}, u32[]{:S(2)}) copy-start(f32[128]{0:T(128)} %get-tuple-element.140) | copy-start | bytes 1540
  207.2 6.8 %copy-start.35 = (f32[128]{0:T(128)S(1)}, f32[128]{0:T(128)}, u32[]{:S(2)}) copy-start(f32[128]{0:T(128)} %get-tuple-element.141) | copy-start | bytes 1540
  207.2 6.8 %copy-start.36 = (f32[128]{0:T(128)S(1)}, f32[128]{0:T(128)}, u32[]{:S(2)}) copy-start(f32[128]{0:T(128)} %get-tuple-element.142) | copy-start | bytes 1540
  207.2 6.8 %copy-start.37 = (f32[128]{0:T(128)S(1)}, f32[128]{0:T(128)}, u32[]{:S(2)}) copy-start(f32[128]{0:T(128)} %get-tuple-element.143) | copy-start | bytes 1540
  207.2 6.8 %copy-start.38 = (f32[128]{0:T(128)S(1)}, f32[128]{0:T(128)}, u32[]{:S(2)}) copy-start(f32[128]{0:T(128)} %get-tuple-element.144) | copy-start | bytes 1540
  209.2 4.5 %collective-permute-start.7 = (bf16[30,128]{1,0:T(8,128)(2,1)S(1)}, bf16[30,128]{1,0:T(8,128)(2,1)S(1)}, u32[]{:S(2)}, u32[]{:S(2)}) collective-permute-start(bf16[30,128]{1,0:T(8,128)(2,1)S(1)} %slice.369), channel_id=1, source_target_pairs={{0,8},{8,16},{16,24},{24,32},{32,40},{40,48},{48,56},{56,64},{64,7... | collective-permute-start | bytes 23048 | tf_op jit(solution)/shard_map/ppermute | solution.py:97
  216.2 10.2 %all-to-all-start.1 = ((f32[8,1,768]{2,1,0:T(1,128)}), f32[8,1,768]{2,1,0:T(1,128)}, u32[]{:S(2)}, u32[]{:S(2)}) async-start(f32[8,1,768]{2,1,0:T(1,128)} %broadcast_in_dim.93), calls=%async_computation.1 | async-start | bytes 49152 | tf_op jit(solution)/shard_map/all_to_all | solution.py:45
  228.0 17.8 %all-to-all-start = ((bf16[16,129,128]{2,1,0:T(8,128)(2,1)}), bf16[16,129,128]{2,1,0:T(8,128)(2,1)}, u32[]{:S(2)}, u32[]{:S(2)}) async-start(bf16[16,129,128]{2,1,0:T(8,128)(2,1)} %broadcast_in_dim.89), calls=%async_computation | async-start | bytes 1114112 | tf_op jit(solution)/shard_map/all_to_all | solution.py:45
  237.3 11.1 %copy-start.4 = (f32[128,6,128]{0,2,1:T(8,128)S(1)}, f32[128,6,128]{0,2,1:T(8,128)}, u32[]{:S(2)}) copy-start(f32[128,6,128]{0,2,1:T(8,128)} %copy-done.3) | copy-start | bytes 1179652
  237.3 11.6 %copy-start.40 = (f32[128]{0:T(128)S(1)}, f32[128]{0:T(128)}, u32[]{:S(2)}) copy-start(f32[128]{0:T(128)} %param.34) | copy-start | bytes 1540
  245.8 2.7 copy-start.10
  289.5 3.3 %copy-start.1 = (bf16[768,2048]{1,0:T(8,128)(2,1)S(1)}, bf16[768,2048]{1,0:T(8,128)(2,1)}, u32[]{:S(2)}) copy-start(bf16[768,2048]{1,0:T(8,128)(2,1)} %copy-done) | copy-start | bytes 9437188
  (6 other events, 11.0 us)
Sparse Core Ops, SparseCore 0:
  9.4 44.8 all-gather.5
  56.5 57.0 all-gather.3
  115.3 49.7 all-gather.7
